TPU v7x, 32 devices: a whole 2x2x4 slice. The times are simulated.
32 devices in a mesh: rep: 2 (over x), fs: 8 (over z, y), tp: 2 (over core).
Axes of the slice: x: 2, y: 2, z: 4, core: 2. Of those that a mesh axis runs over, the one named last changes fastest.
Arguments:
- states: bfloat16 [6144, 2048], P(('rep', 'fs'), 'tp'), may hold values from -6 to 6
- mix_gain: float32 [2048], replicated, may hold values from 0.1 to 1.9
- w_value: bfloat16 [2048, 2048], P('fs', 'tp'), may hold values from -1 to 1
- w_gate: bfloat16 [2048, 2048], P('fs', 'tp'), may hold values from -0.125 to 0.125
- conv_kernel: float32 [31, 2048], replicated, may hold values from -1 to 1
- chan_gain: float32 [2048], replicated, may hold values from 0.1 to 1.9
- w_mix_out: bfloat16 [2048, 2048], P('fs', 'tp'), may hold values from -0.125 to 0.125
- mlp_gain: float32 [2048], replicated, may hold values from 0.1 to 1.9
- w_up: bfloat16 [2048, 6144], P('fs', 'tp'), may hold values from -0.125 to 0.125
- w_down_t: bfloat16 [2048, 6144], P('fs', 'tp'), may hold values from -0.078125 to 0.078125
Outputs:
- layer_out: bfloat16 [6144, 2048], P(('rep', 'fs'), 'tp')
All inputs are finite; a program needn't handle non-finite values.
Results may differ from a plain program's by a relative error of at most 0.017.
Values may be sent and summed in bfloat16 or wider, within the bound.
A program may use at most 64 MiB of HBM per device.

v0:
```python
import jax
import jax.numpy as jnp
from jax import lax
from jax.sharding import PartitionSpec as P

D = 2048
KWIDTH = 31
LENGTH = 128


EPS = 1e-06


def rms_norm(rows, gain):
    values = rows.astype(jnp.float32)
    scaled = values * lax.rsqrt(jnp.mean(values * values, axis=-1, keepdims=True) + EPS)
    return (scaled * gain).astype(jnp.bfloat16)


def times_transposed(left, right):
    return lax.dot_general(
        left, right, (((1,), (1,)), ((), ())), preferred_element_type=jnp.float32
    )


def body(
    states, mix_gain, w_value, w_gate, conv_kernel, chan_gain, w_mix_out, mlp_gain, w_up, w_down_t
):
    width = states.shape[1]
    offset = lax.axis_index("tp") * width
    token_rows = states.shape[0]
    whole_rows = lax.all_gather(states, "tp", axis=1, tiled=True)
    normed = rms_norm(whole_rows, mix_gain)
    columns = normed
    value = jnp.dot(
        columns,
        lax.all_gather(w_value, "fs", axis=0, tiled=True),
        preferred_element_type=jnp.float32,
    )
    gate = jnp.dot(
        columns,
        lax.all_gather(w_gate, "fs", axis=0, tiled=True),
        preferred_element_type=jnp.float32,
    )
    gated = value * jax.nn.sigmoid(gate)
    own_kernel = lax.dynamic_slice_in_dim(conv_kernel, offset, width, 1)
    blocks = gated.reshape(token_rows // LENGTH, LENGTH, width)
    padded = jnp.pad(blocks, ((0, 0), (KWIDTH - 1, 0), (0, 0)))
    filtered = jnp.zeros_like(blocks)
    for tap in range(KWIDTH):
        filtered = filtered + own_kernel[tap][None, None, :] * padded[:, tap : tap + LENGTH, :]
    filtered = filtered.reshape(token_rows, width)
    sum_rows, square_rows = lax.psum(
        (jnp.sum(filtered, axis=-1), jnp.sum(filtered * filtered, axis=-1)), "tp"
    )
    mean_rows = (sum_rows / D)[:, None]
    variance = (square_rows / D)[:, None] - mean_rows * mean_rows
    own_gain = lax.dynamic_slice_in_dim(chan_gain, offset, width, 0)
    activated = jax.nn.silu((filtered - mean_rows) * lax.rsqrt(variance + EPS) * own_gain).astype(
        jnp.bfloat16
    )
    mixer_terms = times_transposed(activated, lax.all_gather(w_mix_out, "fs", axis=0, tiled=True))
    mixed = lax.psum_scatter(
        mixer_terms.astype(jnp.bfloat16), "tp", scatter_dimension=1, tiled=True
    ).astype(jnp.float32)
    middle = (states.astype(jnp.float32) + mixed).astype(jnp.bfloat16)
    middle_rows = lax.all_gather(middle, "tp", axis=1, tiled=True)
    normed_mid = rms_norm(middle_rows, mlp_gain)
    columns = normed_mid
    upward = jnp.dot(
        columns, lax.all_gather(w_up, "fs", axis=0, tiled=True), preferred_element_type=jnp.float32
    )
    hidden = jnp.square(jnp.maximum(upward, 0.0)).astype(jnp.bfloat16)
    fed_terms = times_transposed(hidden, lax.all_gather(w_down_t, "fs", axis=0, tiled=True))
    fed = lax.psum_scatter(
        fed_terms.astype(jnp.bfloat16), "tp", scatter_dimension=1, tiled=True
    ).astype(jnp.float32)
    return (middle.astype(jnp.float32) + fed).astype(jnp.bfloat16)


def solution(mesh):
    in_specs = (
        P(("rep", "fs"), "tp"),
        P(),
        P("fs", "tp"),
        P("fs", "tp"),
        P(),
        P(),
        P("fs", "tp"),
        P(),
        P("fs", "tp"),
        P("fs", "tp"),
    )
    out_specs = P(("rep", "fs"), "tp")
    return jax.shard_map(body, mesh=mesh, in_specs=in_specs, out_specs=out_specs, check_vma=False)
```

profile of v0, /device:TPU:0, one launch (start us, length us, event | category | flops | bytes accessed | tf_op | source)
XLA Modules:
  0.0 658.4 jit_solution(12516439432388913050)
XLA Ops:
  6.5 0.7 all-gather.8.cloned.1.call-update
  7.3 0.7 all-gather.12.cloned.1.call-update
  8.1 0.7 all-gather.10.cloned.1.call-update
  8.8 0.5 all-gather.14.cloned.1.call-update
  9.3 0.0 reduce-scatter.3.cloned.1.call-start
  9.4 1.3 fusion.79
  10.7 1.5 constant_dynamic-slice_fusion
  12.2 9.2 %all-gather.8.cloned.1.call-done = bf16[384,2048]{1,0:T(8,128)(2,1)} async-done(((bf16[384,1024]{1,0:T(8,128)(2,1)}), bf16[384,2048]{1,0:T(8,128)(2,1)}) %all-gather.8.cloned.1.call-update) | async-done | bytes 1572880 | tf_op jit(solution)/shard_map/all_gather | solution.py:32
  21.4 1.9 fusion
  23.4 74.2 %all-gather.12.cloned.1.call-done = bf16[2048,1024]{1,0:T(8,128)(2,1)} async-done(((bf16[256,1024]{1,0:T(8,128)(2,1)}), bf16[2048,1024]{1,0:T(8,128)(2,1)}) %all-gather.12.cloned.1.call-update) | async-done | bytes 4194320 | tf_op jit(solution)/shard_map/all_gather | solution.py:42
  97.6 4.0 fusion.73
  101.6 69.5 %all-gather.10.cloned.1.call-done = bf16[2048,1024]{1,0:T(8,128)(2,1)} async-done(((bf16[256,1024]{1,0:T(8,128)(2,1)}), bf16[2048,1024]{1,0:T(8,128)(2,1)}) %all-gather.10.cloned.1.call-update) | async-done | bytes 4194320 | tf_op jit(solution)/shard_map/all_gather | solution.py:37
  171.0 4.1 divide_multiply_fusion
  175.2 7.0 %fusion.77 = (f32[3,128]{1,0:T(4,128)S(1)}, f32[3,128]{1,0:T(4,128)S(1)}, f32[3,128,1024]{2,1,0:T(8,128)S(1)}) fusion(f32[3,128,1024]{2,1,0:T(8,128)S(1)} %bitcast.48, f32[1024]{0:T(1024)S(1)} %bitcast.61, f32[1024]{0:T(1024)S(1)} %bitcast.63, f32[1024]{0:T(1024)S(1)} %bitcast.64, f32[1024]{0:T(1024)S(1)} %bitcast.65, f32[1024]{0:T(1024)S(1)} %bitcast.66, ...), kind=kLoop, calls=%fused_computation.120 | loop fusion | flops 25165056 | bytes 3275776 | tf_op jit(solution)/shard_map/reduce_sum | solution.py:54
  182.2 2.5 all-reduce.1
  184.7 0.6 multiply_convert_fusion.1
  185.2 59.1 %all-gather.14.cloned.1.call-done = bf16[2048,1024]{1,0:T(8,128)(2,1)} async-done(((bf16[256,1024]{1,0:T(8,128)(2,1)}), bf16[2048,1024]{1,0:T(8,128)(2,1)}) %all-gather.14.cloned.1.call-update) | async-done | bytes 4194320 | tf_op jit(solution)/shard_map/all_gather | solution.py:62
  244.4 5.2 convolution_convert_fusion
  249.6 0.0 all-gather.16.cloned.1.call-start
  249.7 7.6 %reduce-scatter.3.cloned.1.call-done = bf16[384,1024]{1,0:T(8,128)(2,1)} async-done(((bf16[384,2048]{1,0:T(8,128)(2,1)}), bf16[384,1024]{1,0:T(8,128)(2,1)}) %reduce-scatter.3.cloned.1.call-update) | async-done | bytes 786448 | tf_op jit(solution)/shard_map/reduce_scatter | solution.py:63
  257.3 2.3 add_convert_fusion.1
  259.6 0.0 all-gather.18.cloned.1.call-start
  259.6 0.7 all-gather.18.cloned.1.call-update
  260.4 0.7 all-gather.20.cloned.1.call-update
  261.1 0.2 reduce-scatter.5.cloned.1.call-start
  261.3 9.5 %all-gather.16.cloned.1.call-done = bf16[384,2048]{1,0:T(8,128)(2,1)} async-done(((bf16[384,1024]{1,0:T(8,128)(2,1)}), bf16[384,2048]{1,0:T(8,128)(2,1)}) %all-gather.16.cloned.1.call-update) | async-done | bytes 1572880 | tf_op jit(solution)/shard_map/all_gather | solution.py:67
  270.8 1.9 fusion.3
  272.8 177.6 %all-gather.18.cloned.1.call-done = bf16[2048,3072]{1,0:T(8,128)(2,1)} async-done(((bf16[256,3072]{1,0:T(8,128)(2,1)}), bf16[2048,3072]{1,0:T(8,128)(2,1)}) %all-gather.18.cloned.1.call-update) | async-done | bytes 12582928 | tf_op jit(solution)/shard_map/all_gather | solution.py:71
  450.3 176.5 %all-gather.20.cloned.1.call-done = bf16[2048,3072]{1,0:T(8,128)(2,1)} async-done(((bf16[256,3072]{1,0:T(8,128)(2,1)}), bf16[2048,3072]{1,0:T(8,128)(2,1)}) %all-gather.20.cloned.1.call-update) | async-done | bytes 12582928 | tf_op jit(solution)/shard_map/all_gather | solution.py:74
  626.8 15.3 %convolution_convert_fusion.1 = bf16[384,2048]{1,0:T(8,128)(2,1)} fusion(bf16[2048,3072]{1,0:T(8,128)(2,1)} %all-gather.20.cloned.1.call-done, bf16[2048,3072]{1,0:T(8,128)(2,1)} %all-gather.18.cloned.1.call-done, bf16[384,2048]{1,0:T(8,128)(2,1)S(1)} %copy-done.3, f32[2048]{0:T(1024)S(1)} %copy-done.5, f32[384]{0:T(512)S(1)} %add_rsqrt_fusion), kind=kOutput, calls=%fused_computation.42 | convolution fusion | flops 9671147520 | bytes 28321280 | tf_op jit(solution)/shard_map/dot_general | solution.py:21
  642.2 7.3 %reduce-scatter.5.cloned.1.call-done = bf16[384,1024]{1,0:T(8,128)(2,1)} async-done(((bf16[384,2048]{1,0:T(8,128)(2,1)}), bf16[384,1024]{1,0:T(8,128)(2,1)}) %reduce-scatter.5.cloned.1.call-update) | async-done | bytes 786448 | tf_op jit(solution)/shard_map/reduce_scatter | solution.py:75
  649.5 2.3 add_convert_fusion
  (25 shorter events, 0.3 us)
Async XLA Ops:
  6.5 14.9 %all-gather.8.cloned.1.call-start = ((), (), s32[]{:S(2)}) async-start(), calls=%async_computation.2 | async-start | bytes 2359296 | tf_op jit(solution)/shard_map/all_gather | solution.py:32
  7.3 90.3 %all-gather.12.cloned.1.call-start = ((), (), s32[]{:S(2)}) async-start(), calls=%async_computation.4 | async-start | bytes 4718592 | tf_op jit(solution)/shard_map/all_gather | solution.py:42
  8.0 89.6 %copy-start.4 = (f32[2048]{0:T(1024)S(1)}, f32[2048]{0:T(1024)}, u32[]{:S(2)}) copy-start(f32[2048]{0:T(1024)} %param.11) | copy-start | bytes 24580
  8.0 163.0 %all-gather.10.cloned.1.call-start = ((), (), s32[]{:S(2)}) async-start(), calls=%async_computation.3 | async-start | bytes 4718592 | tf_op jit(solution)/shard_map/all_gather | solution.py:37
  8.8 235.6 %all-gather.14.cloned.1.call-start = ((), (), s32[]{:S(2)}) async-start(), calls=%async_computation.5 | async-start | bytes 4718592 | tf_op jit(solution)/shard_map/all_gather | solution.py:62
  9.3 247.9 %reduce-scatter.3.cloned.1.call-start = ((), (), s32[]{:S(2)}) async-start(), calls=%async_computation.6 | async-start | bytes 2359296 | tf_op jit(solution)/shard_map/reduce_scatter | solution.py:63
  21.4 76.1 %copy-start.2 = (bf16[384,2048]{1,0:T(8,128)(2,1)S(1)}, bf16[384,2048]{1,0:T(8,128)(2,1)}, u32[]{:S(2)}) copy-start(bf16[384,2048]{1,0:T(8,128)(2,1)} %all-gather.8.cloned.1.call-done) | copy-start | bytes 4718596
  175.2 9.5 %dynamic-slice-start = ((f32[2048]{0:T(1024)}, s32[]{:T(128)}), f32[1024]{0:T(1024)S(1)}, s32[]{:S(2)}) async-start(f32[2048]{0:T(1024)} %param.15, s32[]{:T(128)} %select_n.4), calls=%async_computation.11 | async-start | bytes 8704 | tf_op jit(solution)/shard_map/dynamic_slice | solution.py:58
  249.6 7.7 %copy-start.1 = (bf16[384,1024]{1,0:T(8,128)(2,1)S(1)}, bf16[384,1024]{1,0:T(8,128)(2,1)}, u32[]{:S(2)}) copy-start(bf16[384,1024]{1,0:T(8,128)(2,1)} %param.10) | copy-start | bytes 2359300
  249.6 21.2 %all-gather.16.cloned.1.call-start = ((), (), s32[]{:S(2)}) async-start(), calls=%async_computation.7 | async-start | bytes 2359296 | tf_op jit(solution)/shard_map/all_gather | solution.py:67
  259.6 190.7 %all-gather.18.cloned.1.call-start = ((), (), s32[]{:S(2)}) async-start(), calls=%async_computation.8 | async-start | bytes 14155776 | tf_op jit(solution)/shard_map/all_gather | solution.py:71
  260.3 366.5 %copy-start.5 = (f32[2048]{0:T(1024)S(1)}, f32[2048]{0:T(1024)}, u32[]{:S(2)}) copy-start(f32[2048]{0:T(1024)} %param.17) | copy-start | bytes 24580
  260.4 366.5 %all-gather.20.cloned.1.call-start = ((), (), s32[]{:S(2)}) async-start(), calls=%async_computation.9 | async-start | bytes 14155776 | tf_op jit(solution)/shard_map/all_gather | solution.py:74
  261.1 388.4 %reduce-scatter.5.cloned.1.call-start = ((), (), s32[]{:S(2)}) async-start(), calls=%async_computation.10 | async-start | bytes 2359296 | tf_op jit(solution)/shard_map/reduce_scatter | solution.py:75
  270.8 356.0 %copy-start.3 = (bf16[384,2048]{1,0:T(8,128)(2,1)S(1)}, bf16[384,2048]{1,0:T(8,128)(2,1)}, u32[]{:S(2)}) copy-start(bf16[384,2048]{1,0:T(8,128)(2,1)} %all-gather.16.cloned.1.call-done) | copy-start | bytes 4718596
  642.2 7.3 %copy-start = (bf16[384,1024]{1,0:T(8,128)(2,1)S(1)}, bf16[384,1024]{1,0:T(8,128)(2,1)}, u32[]{:S(2)}) copy-start(bf16[384,1024]{1,0:T(8,128)(2,1)} %add_convert_fusion.1) | copy-start | bytes 2359300
Sparse Core Ops, SparseCore 0:
  8.9 12.5 all-gather.7
  23.6 73.9 all-gather.11
  99.7 71.3 all-gather.9
  173.0 71.3 all-gather.13
  249.7 7.4 reduce-scatter.2
  259.7 11.0 all-gather.15
  273.0 177.2 all-gather.17
  452.5 174.2 all-gather.19
  642.3 7.1 reduce-scatter.4
where the time goes:
time: 659 us; the launch traced here: 658 us
  waiting for transfers between devices  594 us (90%)
  matrix products  28.7 us (4%)
  other arithmetic  16.1 us (2%)
  between operations  13.3 us (2%)
    all_gather x1, waiting for transfers between devices, body(): lax.all_gather(w_up, 'fs', axis=0, tiled=True)  178 us
    all_gather x1, waiting for transfers between devices, body(): lax.all_gather(w_down_t, 'fs', axis=0, tiled=True)  176 us
    all_gather x1, waiting for transfers between devices, body(): lax.all_gather(w_gate, 'fs', axis=0, tiled=True)  74.2 us
    all_gather x1, waiting for transfers between devices, body(): lax.all_gather(w_value, 'fs', axis=0, tiled=True)  69.5 us
    all_gather x1, waiting for transfers between devices, body(): lax.all_gather(w_mix_out, 'fs', axis=0, tiled=True)  59.1 us
    dot_general x2, matrix products, times_transposed(): lax.dot_general(left, right, (((1,), (1,)), ((), ())), preferred_element_...  20.6 us
  transfers between devices with their start and end apart: 9, of which 9 were waited for; matrix products, arithmetic and copies ran while one was open for 3% of the time, Pallas kernels for 0%

commit v1 on v0

v1 whole, which is shorter than its diff:
```python
import jax
import jax.numpy as jnp
from jax import lax
from jax.sharding import PartitionSpec as P

D = 2048
KWIDTH = 31
LENGTH = 128


EPS = 1e-06


def rms_norm(rows, gain):
    values = rows.astype(jnp.float32)
    scaled = values * lax.rsqrt(jnp.mean(values * values, axis=-1, keepdims=True) + EPS)
    return (scaled * gain).astype(jnp.bfloat16)


def times_transposed(left, right):
    return lax.dot_general(
        left, right, (((1,), (1,)), ((), ())), preferred_element_type=jnp.float32
    )


def body(
    states, mix_gain, w_value, w_gate, conv_kernel, chan_gain, w_mix_out, mlp_gain, w_up, w_down_t
):
    reps = lax.axis_size("rep")
    rep = lax.axis_index("rep")
    own_width = states.shape[1]
    width = own_width // reps
    offset = lax.axis_index("tp") * own_width + rep * width
    channels = own_width * lax.axis_size("tp")

    def own_columns(weight):
        part = weight.shape[1] // reps
        piece = lax.dynamic_slice_in_dim(weight, rep * part, part, 1)
        return lax.all_gather(piece, "fs", axis=0, tiled=True)

    def all_rows(rows):
        return lax.all_gather(
            lax.all_gather(rows, "tp", axis=1, tiled=True), "rep", axis=0, tiled=True
        )

    def own_sums(terms):
        terms = lax.psum_scatter(
            terms.astype(jnp.bfloat16), "rep", scatter_dimension=0, tiled=True
        )
        return lax.psum_scatter(terms, "tp", scatter_dimension=1, tiled=True).astype(jnp.float32)

    normed = rms_norm(all_rows(states), mix_gain)
    token_rows = normed.shape[0]
    value = jnp.dot(normed, own_columns(w_value), preferred_element_type=jnp.float32)
    gate = jnp.dot(normed, own_columns(w_gate), preferred_element_type=jnp.float32)
    gated = value * jax.nn.sigmoid(gate)
    own_kernel = lax.dynamic_slice_in_dim(conv_kernel, offset, width, 1)
    blocks = gated.reshape(token_rows // LENGTH, LENGTH, width)
    padded = jnp.pad(blocks, ((0, 0), (KWIDTH - 1, 0), (0, 0)))
    filtered = jnp.zeros_like(blocks)
    for tap in range(KWIDTH):
        filtered = filtered + own_kernel[tap][None, None, :] * padded[:, tap : tap + LENGTH, :]
    filtered = filtered.reshape(token_rows, width)
    sum_rows, square_rows = lax.psum(
        (jnp.sum(filtered, axis=-1), jnp.sum(filtered * filtered, axis=-1)), ("rep", "tp")
    )
    mean_rows = (sum_rows / channels)[:, None]
    variance = (square_rows / channels)[:, None] - mean_rows * mean_rows
    own_gain = lax.dynamic_slice_in_dim(chan_gain, offset, width, 0)
    activated = jax.nn.silu((filtered - mean_rows) * lax.rsqrt(variance + EPS) * own_gain).astype(
        jnp.bfloat16
    )
    mixed = own_sums(times_transposed(activated, own_columns(w_mix_out)))
    middle = (states.astype(jnp.float32) + mixed).astype(jnp.bfloat16)
    normed_mid = rms_norm(all_rows(middle), mlp_gain)
    upward = jnp.dot(normed_mid, own_columns(w_up), preferred_element_type=jnp.float32)
    hidden = jnp.square(jnp.maximum(upward, 0.0)).astype(jnp.bfloat16)
    fed = own_sums(times_transposed(hidden, own_columns(w_down_t)))
    return (middle.astype(jnp.float32) + fed).astype(jnp.bfloat16)


def solution(mesh):
    in_specs = (
        P(("rep", "fs"), "tp"),
        P(),
        P("fs", "tp"),
        P("fs", "tp"),
        P(),
        P(),
        P("fs", "tp"),
        P(),
        P("fs", "tp"),
        P("fs", "tp"),
    )
    out_specs = P(("rep", "fs"), "tp")
    return jax.shard_map(body, mesh=mesh, in_specs=in_specs, out_specs=out_specs, check_vma=False)
```

time: 659 us -> 619 us (0.939)
  waiting for transfers between devices: 594 us -> 540 us
    all_gather x7 -> x9, waiting for transfers between devices: 576 us -> 433 us  [the longest x5 321 us: own_columns(): return lax.all_gather(piece, 'fs', axis=0, tiled=True)]
    reduce_scatter x2 -> x4, waiting for transfers between devices: 14.9 us -> 106 us  [the longest x2 83.8 us: own_sums(): lax.psum_scatter(terms.astype(jnp.bfloat16), 'rep', scatter_dimension=0,...]
  transfers between devices with their start and end apart: 9 -> 13, of which waited for: 9 -> 13; matrix products, arithmetic and copies ran while one was open for 3% -> 5% of each run, Pallas kernels for 0% -> 0%
where the time goes in v1:
time: 619 us; the launch traced here: 618 us
  waiting for transfers between devices  540 us (87%)
  matrix products  32.9 us (5%)
  other arithmetic  17.6 us (3%)
  between operations  13.4 us (2%)
  local copies, waits for them, and re-layouts  7.93 us (1%)
    all_gather x5, waiting for transfers between devices, own_columns(): return lax.all_gather(piece, 'fs', axis=0, tiled=True)  321 us
    all_gather x2, waiting for transfers between devices, all_rows(): lax.all_gather(lax.all_gather(rows, 'tp', axis=1, tiled=True), 'rep', axi...  86.6 us
    reduce_scatter x2, waiting for transfers between devices, own_sums(): lax.psum_scatter(terms.astype(jnp.bfloat16), 'rep', scatter_dimension=0,...  83.8 us
    all_gather x2, waiting for transfers between devices, all_rows(): lax.all_gather(rows, 'tp', axis=1, tiled=True)  25.3 us
    dot_general x2, matrix products, times_transposed(): lax.dot_general(left, right, (((1,), (1,)), ((), ())), preferred_element_...  22.4 us
    reduce_scatter x2, waiting for transfers between devices, own_sums(): lax.psum_scatter(terms, 'tp', scatter_dimension=1, tiled=True)  22.4 us
  transfers between devices with their start and end apart: 13, of which 13 were waited for; matrix products, arithmetic and copies ran while one was open for 5% of the time, Pallas kernels for 0%

profile of v1, /device:TPU:0, one launch (start us, length us, event | category | flops | bytes accessed | tf_op | source)
XLA Modules:
  0.0 618.3 jit_solution(12692080250900733453)
XLA Ops:
  7.3 14.1 %all-gather.10.cloned.1.call-done = bf16[384,2048]{1,0:T(8,128)(2,1)} async-done(((bf16[384,1024]{1,0:T(8,128)(2,1)}), bf16[384,2048]{1,0:T(8,128)(2,1)}) %all-gather.10.cloned.1.call-update) | async-done | bytes 1572880 | tf_op jit(solution)/shard_map/all_gather | solution.py:43
  21.5 0.7 constant_dynamic-slice_fusion.5
  22.3 0.7 constant_dynamic-slice_fusion.4
  23.2 0.7 constant_dynamic-slice_fusion.3
  24.0 0.8 dynamic_slice.24
  24.7 1.1 fusion.79
  25.8 1.4 constant_dynamic-slice_fusion
  27.2 41.9 %all-gather.12.cloned.1.call-done = bf16[768,2048]{1,0:T(8,128)(2,1)} async-done(((bf16[384,2048]{1,0:T(8,128)(2,1)}), bf16[768,2048]{1,0:T(8,128)(2,1)}) %all-gather.12.cloned.1.call-update) | async-done | bytes 3145744 | tf_op jit(solution)/shard_map/all_gather | solution.py:42
  69.1 2.6 fusion
  71.7 48.7 %all-gather.14.cloned.1.call-done = bf16[2048,512]{1,0:T(8,128)(2,1)} async-done(((bf16[256,512]{1,0:T(8,128)(2,1)}), bf16[2048,512]{1,0:T(8,128)(2,1)}) %all-gather.14.cloned.1.call-update) | async-done | bytes 2097168 | tf_op jit(solution)/shard_map/all_gather | solution.py:39
  120.3 5.5 fusion.72
  125.9 44.1 %all-gather.16.cloned.1.call-done = bf16[2048,512]{1,0:T(8,128)(2,1)} async-done(((bf16[256,512]{1,0:T(8,128)(2,1)}), bf16[2048,512]{1,0:T(8,128)(2,1)}) %all-gather.16.cloned.1.call-update) | async-done | bytes 2097168 | tf_op jit(solution)/shard_map/all_gather | solution.py:39
  170.0 5.0 divide_multiply_fusion
  175.0 6.4 %fusion.77 = (f32[6,128]{1,0:T(8,128)S(1)}, f32[6,128]{1,0:T(8,128)S(1)}, f32[6,128,512]{2,1,0:T(8,128)S(1)}) fusion(f32[6,128,512]{2,1,0:T(8,128)S(1)} %bitcast.48, f32[512]{0:T(512)S(1)} %bitcast.63, f32[512]{0:T(512)S(1)} %bitcast.65, f32[512]{0:T(512)S(1)} %bitcast.66, f32[512]{0:T(512)S(1)} %bitcast.67, f32[512]{0:T(512)S(1)} %bitcast.68, ...), kind=kLoop, calls=%fused_computation.125 | loop fusion | flops 25164288 | bytes 3215360 | tf_op jit(solution)/shard_map/reduce_sum | solution.py:65
  181.4 6.0 all-reduce.1
  187.4 1.4 multiply_convert_fusion.1
  188.8 30.8 %all-gather.18.cloned.1.call-done = bf16[2048,512]{1,0:T(8,128)(2,1)} async-done(((bf16[256,512]{1,0:T(8,128)(2,1)}), bf16[2048,512]{1,0:T(8,128)(2,1)}) %all-gather.18.cloned.1.call-update) | async-done | bytes 2097168 | tf_op jit(solution)/shard_map/all_gather | solution.py:39
  219.6 5.3 convolution_convert_fusion
  225.0 42.0 %reduce-scatter.5.cloned.1.call-done = bf16[384,2048]{1,0:T(8,128)(2,1)} async-done(((bf16[768,2048]{1,0:T(8,128)(2,1)}), bf16[384,2048]{1,0:T(8,128)(2,1)}) %reduce-scatter.5.cloned.1.call-update) | async-done | bytes 1572880 | tf_op jit(solution)/shard_map/reduce_scatter | solution.py:47
  267.1 11.2 %reduce-scatter.7.cloned.1.call-done = bf16[384,1024]{1,0:T(8,128)(2,1)} async-done(((bf16[384,2048]{1,0:T(8,128)(2,1)}), bf16[384,1024]{1,0:T(8,128)(2,1)}) %reduce-scatter.7.cloned.1.call-update) | async-done | bytes 786448 | tf_op jit(solution)/shard_map/reduce_scatter | solution.py:50
  278.3 2.3 add_convert_fusion.1
  280.7 11.2 %all-gather.20.cloned.1.call-done = bf16[384,2048]{1,0:T(8,128)(2,1)} async-done(((bf16[384,1024]{1,0:T(8,128)(2,1)}), bf16[384,2048]{1,0:T(8,128)(2,1)}) %all-gather.20.cloned.1.call-update) | async-done | bytes 1572880 | tf_op jit(solution)/shard_map/all_gather | solution.py:43
  291.9 1.0 constant_dynamic-slice_fusion.2
  293.6 0.9 constant_dynamic-slice_fusion.1
  294.8 44.7 %all-gather.22.cloned.1.call-done = bf16[768,2048]{1,0:T(8,128)(2,1)} async-done(((bf16[384,2048]{1,0:T(8,128)(2,1)}), bf16[768,2048]{1,0:T(8,128)(2,1)}) %all-gather.22.cloned.1.call-update) | async-done | bytes 3145744 | tf_op jit(solution)/shard_map/all_gather | solution.py:42
  339.5 2.6 fusion.3
  342.1 98.2 %all-gather.24.cloned.1.call-done = bf16[2048,1536]{1,0:T(8,128)(2,1)} async-done(((bf16[256,1536]{1,0:T(8,128)(2,1)}), bf16[2048,1536]{1,0:T(8,128)(2,1)}) %all-gather.24.cloned.1.call-update) | async-done | bytes 6291472 | tf_op jit(solution)/shard_map/all_gather | solution.py:39
  440.3 99.1 %all-gather.26.cloned.1.call-done = bf16[2048,1536]{1,0:T(8,128)(2,1)} async-done(((bf16[256,1536]{1,0:T(8,128)(2,1)}), bf16[2048,1536]{1,0:T(8,128)(2,1)}) %all-gather.26.cloned.1.call-update) | async-done | bytes 6291472 | tf_op jit(solution)/shard_map/all_gather | solution.py:39
  539.4 17.1 %convolution_convert_fusion.1 = bf16[768,2048]{1,0:T(8,128)(2,1)} fusion(bf16[2048,1536]{1,0:T(8,128)(2,1)} %all-gather.26.cloned.1.call-done, bf16[2048,1536]{1,0:T(8,128)(2,1)} %all-gather.24.cloned.1.call-done, bf16[768,2048]{1,0:T(8,128)(2,1)} %all-gather.22.cloned.1.call-done, f32[2048]{0:T(1024)S(1)} %copy-done.8, f32[768]{0:T(1024)S(1)} %add_rsqrt_fusion), kind=kOutput, calls=%fused_computation.42 | convolution fusion | flops 9675079680 | bytes 18885632 | tf_op jit(solution)/shard_map/dot_general | solution.py:21
  556.5 41.7 %reduce-scatter.9.cloned.1.call-done = bf16[384,2048]{1,0:T(8,128)(2,1)} async-done(((bf16[768,2048]{1,0:T(8,128)(2,1)}), bf16[384,2048]{1,0:T(8,128)(2,1)}) %reduce-scatter.9.cloned.1.call-update) | async-done | bytes 1572880 | tf_op jit(solution)/shard_map/reduce_scatter | solution.py:47
  598.3 11.2 %reduce-scatter.11.cloned.1.call-done = bf16[384,1024]{1,0:T(8,128)(2,1)} async-done(((bf16[384,2048]{1,0:T(8,128)(2,1)}), bf16[384,1024]{1,0:T(8,128)(2,1)}) %reduce-scatter.11.cloned.1.call-update) | async-done | bytes 786448 | tf_op jit(solution)/shard_map/reduce_scatter | solution.py:50
  609.5 2.3 add_convert_fusion
  (47 shorter events, 2.2 us)
Async XLA Ops:
  6.5 285.4 %copy-start = (bf16[256,3072]{1,0:T(8,128)(2,1)S(1)}, bf16[256,3072]{1,0:T(8,128)(2,1)}, u32[]{:S(2)}) copy-start(bf16[256,3072]{1,0:T(8,128)(2,1)} %param.18) | copy-start | bytes 4718596
  6.5 15.0 %copy-start.4 = (bf16[256,1024]{1,0:T(8,128)(2,1)S(1)}, bf16[256,1024]{1,0:T(8,128)(2,1)}, u32[]{:S(2)}) copy-start(bf16[256,1024]{1,0:T(8,128)(2,1)} %param.12) | copy-start | bytes 1572868
  6.5 15.8 %copy-start.5 = (bf16[256,1024]{1,0:T(8,128)(2,1)S(1)}, bf16[256,1024]{1,0:T(8,128)(2,1)}, u32[]{:S(2)}) copy-start(bf16[256,1024]{1,0:T(8,128)(2,1)} %param.13) | copy-start | bytes 1572868
  6.5 14.9 %all-gather.10.cloned.1.call-start = ((), (), s32[]{:S(2)}) async-start(), calls=%async_computation.4 | async-start | bytes 2359296 | tf_op jit(solution)/shard_map/all_gather | solution.py:43
  7.3 61.8 %all-gather.12.cloned.1.call-start = ((), (), s32[]{:S(2)}) async-start(), calls=%async_computation.5 | async-start | bytes 4718592 | tf_op jit(solution)/shard_map/all_gather | solution.py:42
  21.4 1.7 copy-start.6
  21.5 98.9 %all-gather.14.cloned.1.call-start = ((), (), s32[]{:S(2)}) async-start(), calls=%async_computation.6 | async-start | bytes 2359296 | tf_op jit(solution)/shard_map/all_gather | solution.py:39
  22.3 147.7 %all-gather.16.cloned.1.call-start = ((), (), s32[]{:S(2)}) async-start(), calls=%async_computation.7 | async-start | bytes 2359296 | tf_op jit(solution)/shard_map/all_gather | solution.py:39
  23.1 196.5 %all-gather.18.cloned.1.call-start = ((), (), s32[]{:S(2)}) async-start(), calls=%async_computation.8 | async-start | bytes 2359296 | tf_op jit(solution)/shard_map/all_gather | solution.py:39
  23.9 243.1 %reduce-scatter.5.cloned.1.call-start = ((), (), s32[]{:S(2)}) async-start(), calls=%async_computation.9 | async-start | bytes 4718592 | tf_op jit(solution)/shard_map/reduce_scatter | solution.py:47
  27.2 93.1 %copy-start.7 = (f32[2048]{0:T(1024)S(1)}, f32[2048]{0:T(1024)}, u32[]{:S(2)}) copy-start(f32[2048]{0:T(1024)} %param.11) | copy-start | bytes 24580
  224.9 53.3 %copy-start.2 = (bf16[384,1024]{1,0:T(8,128)(2,1)S(1)}, bf16[384,1024]{1,0:T(8,128)(2,1)}, u32[]{:S(2)}) copy-start(bf16[384,1024]{1,0:T(8,128)(2,1)} %param.10) | copy-start | bytes 2359300
  224.9 53.3 %reduce-scatter.7.cloned.1.call-start = ((), (), s32[]{:S(2)}) async-start(), calls=%async_computation.10 | async-start | bytes 2359296 | tf_op jit(solution)/shard_map/reduce_scatter | solution.py:50
  267.1 24.8 %all-gather.20.cloned.1.call-start = ((), (), s32[]{:S(2)}) async-start(), calls=%async_computation.11 | async-start | bytes 2359296 | tf_op jit(solution)/shard_map/all_gather | solution.py:43
  280.6 58.9 %all-gather.22.cloned.1.call-start = ((), (), s32[]{:S(2)}) async-start(), calls=%async_computation.12 | async-start | bytes 4718592 | tf_op jit(solution)/shard_map/all_gather | solution.py:42
  291.9 1.7 copy-start.3
  291.9 148.4 %all-gather.24.cloned.1.call-start = ((), (), s32[]{:S(2)}) async-start(), calls=%async_computation.13 | async-start | bytes 7077888 | tf_op jit(solution)/shard_map/all_gather | solution.py:39
  292.9 246.4 %all-gather.26.cloned.1.call-start = ((), (), s32[]{:S(2)}) async-start(), calls=%async_computation.14 | async-start | bytes 7077888 | tf_op jit(solution)/shard_map/all_gather | solution.py:39
  294.5 244.8 %copy-start.8 = (f32[2048]{0:T(1024)S(1)}, f32[2048]{0:T(1024)}, u32[]{:S(2)}) copy-start(f32[2048]{0:T(1024)} %param.17) | copy-start | bytes 24580
  294.5 303.7 %reduce-scatter.9.cloned.1.call-start = ((), (), s32[]{:S(2)}) async-start(), calls=%async_computation.15 | async-start | bytes 4718592 | tf_op jit(solution)/shard_map/reduce_scatter | solution.py:47
  556.5 53.0 %copy-start.1 = (bf16[384,1024]{1,0:T(8,128)(2,1)S(1)}, bf16[384,1024]{1,0:T(8,128)(2,1)}, u32[]{:S(2)}) copy-start(bf16[384,1024]{1,0:T(8,128)(2,1)} %add_convert_fusion.1) | copy-start | bytes 2359300
  556.5 53.0 %reduce-scatter.11.cloned.1.call-start = ((), (), s32[]{:S(2)}) async-start(), calls=%async_computation.16 | async-start | bytes 2359296 | tf_op jit(solution)/shard_map/reduce_scatter | solution.py:50
Sparse Core Ops, SparseCore 0:
  8.9 12.5 all-gather.9
  23.0 46.0 all-gather.11
  71.2 49.0 all-gather.13
  122.3 47.6 all-gather.15
  172.0 47.6 all-gather.17
  225.1 41.9 reduce-scatter.4
  269.3 8.9 reduce-scatter.6
  280.8 11.0 all-gather.19
  293.4 46.0 all-gather.21
  341.5 98.6 all-gather.23
  442.5 96.8 all-gather.25
  556.6 41.6 reduce-scatter.8
  600.5 8.9 reduce-scatter.10

commit v2 on v1

v2 whole, which is shorter than its diff:
```python
import functools

import jax
import jax.numpy as jnp
from jax import lax
from jax.experimental import pallas as pl
from jax.experimental.pallas import tpu as pltpu
from jax.sharding import PartitionSpec as P

LENGTH = 128
LANES = 128
LEAD = 32
EPS = 1e-06
MESH = pl.DeviceIdType.MESH


def times_transposed(left, right):
    return lax.dot_general(
        left, right, (((1,), (1,)), ((), ())), preferred_element_type=jnp.float32
    )


def kernel(
    sizes,
    states, mix_gain, w_value, w_gate, conv_kernel, chan_gain, w_mix, mlp_gain, w_up, w_down,
    out,
    weights, rows_in, rows_mid, normed, padded, filtered, activated, hidden,
    own_stats, peer_stats, mix_parts, mix_peers, fed_parts, fed_peers,
    load_sems, ring_send, ring_recv, in_send, in_recv, mid_send, mid_recv,
    stat_send, stat_recv, mix_send, mix_recv, fed_send, fed_recv,
):
    reps, n, tps, rows, channels, width, ups = sizes
    own_width = width * reps
    half_way = n // 2
    shard = channels // n
    tokens = reps * rows
    pieces = tokens // LENGTH
    chunks = 3 + 2 * ups
    rep, fs, tp = lax.axis_index("rep"), lax.axis_index("fs"), lax.axis_index("tp")
    taps = conv_kernel.shape[0]
    blocks, _, block = mix_parts.shape
    per_tp = own_width // block

    def ring_index(place):
        place = lax.rem(place + n, n)
        return jnp.where(place < half_way, 2 * place, 2 * (n - 1 - place) + 1)

    place = jnp.where(lax.rem(fs, 2) == 0, fs // 2, n - 1 - fs // 2)
    neighbours = (ring_index(place + 1), ring_index(place - 1))

    barrier = pltpu.get_barrier_semaphore()
    for other in neighbours:
        pl.semaphore_signal(barrier, inc=1, device_id={"fs": other}, device_id_type=MESH)
    for dr in range(reps):
        for dt in range(tps):
            if dr or dt:
                pl.semaphore_signal(
                    barrier, inc=1,
                    device_id={"rep": lax.rem(rep + dr, reps), "tp": lax.rem(tp + dt, tps)},
                    device_id_type=MESH,
                )
    pl.semaphore_wait(barrier, 1 + reps * tps)

    own_rows = pl.ds(pl.multiple_of(rep * rows, rows), rows)
    own_cols = pl.ds(pl.multiple_of(tp * own_width, own_width), own_width)

    def shard_at(owner, start=0, size=None):
        size = shard if size is None else size
        return pl.ds(pl.multiple_of(owner * shard + start, size), size)

    def hop(c, s, way):
        sign = 1 if way == 0 else -1
        owner = ring_index(place - sign * (s - 1))
        span = shard_at(owner)
        if s == half_way:
            span = shard_at(owner, way * (shard // 2), shard // 2)
        return pltpu.make_async_remote_copy(
            src_ref=weights.at[c, span, :],
            dst_ref=weights.at[c, span, :],
            send_sem=ring_send.at[way, c],
            recv_sem=ring_recv.at[way, c, s - 1],
            device_id={"fs": neighbours[way]},
            device_id_type=MESH,
        )

    loads = []
    for c in range(chunks):
        if c < 3:
            source, column = (w_value, w_gate, w_mix)[c], rep * width
        elif c < 3 + ups:
            source, column = w_up, (rep * ups + c - 3) * width
        else:
            source, column = w_down, (rep * ups + c - 3 - ups) * width
        loads.append(
            pltpu.make_async_copy(
                source.at[:, pl.ds(pl.multiple_of(column, width), width)],
                weights.at[c, shard_at(fs), :],
                load_sems.at[c],
            )
        )
        loads[-1].start()
    own_load = pltpu.make_async_copy(states, rows_in.at[own_rows, own_cols], load_sems.at[chunks])
    own_load.start()

    def pump(c, s):
        for way in range(2):
            if s == 1:
                if way == 0:
                    loads[c].wait()
            else:
                before = hop(c, s - 1, way)
                before.wait_recv()
                before.wait_send()
            hop(c, s, way).start()

    def arrived(c):
        for way in range(2):
            last = hop(c, half_way, way)
            last.wait_recv()
            last.wait_send()

    def spread(source, target, send, recv):
        def copy(dr, dt, ahead):
            if ahead:
                span = pl.ds(pl.multiple_of(lax.rem(rep + reps - dr, reps) * rows, rows), rows)
                src = target.at[span, own_cols]
            else:
                span, src = own_rows, source
            step_r = 0 if ahead else dr
            return pltpu.make_async_remote_copy(
                src_ref=src,
                dst_ref=target.at[span, own_cols],
                send_sem=send.at[dr, dt],
                recv_sem=recv.at[dr, dt],
                device_id={"rep": lax.rem(rep + step_r, reps), "tp": lax.rem(tp + dt, tps)},
                device_id_type=MESH,
            )

        first = [copy(dr, 0, False) for dr in range(1, reps)]
        near = [copy(0, dt, False) for dt in range(1, tps)]
        for one in first + near:
            one.start()

        def forward():
            later = []
            for dr in range(1, reps):
                first[dr - 1].wait_recv()
                for dt in range(1, tps):
                    one = copy(dr, dt, True)
                    one.start()
                    later.append(one)
            return later

        def finish(later):
            for one in near + later:
                one.wait_recv()
            for one in first + near + later:
                one.wait_send()

        return forward, finish

    def norm_all(source, gain):
        def one(i, carry):
            span = pl.ds(pl.multiple_of(i * 64, 64), 64)
            x = source[span, :].astype(jnp.float32)
            scale = lax.rsqrt(jnp.mean(x * x, axis=-1, keepdims=True) + EPS)
            normed[span, :] = (x * scale * gain[...]).astype(jnp.bfloat16)
            return carry

        lax.fori_loop(0, tokens // 64, one, 0)

    def seq_rows(i):
        return pl.ds(pl.multiple_of(i * LENGTH, LENGTH), LENGTH)

    def mixer_rows(i):
        x = normed[seq_rows(i), :]
        value = jnp.dot(x, weights[0], preferred_element_type=jnp.float32)
        gate = jnp.dot(x, weights[1], preferred_element_type=jnp.float32)
        padded[LEAD : LEAD + LENGTH, :] = value * jax.nn.sigmoid(gate)

        def column(j, sums):
            cols = pl.ds(pl.multiple_of(j * LANES, LANES), LANES)
            from_all = pl.multiple_of(tp * own_width + rep * width + j * LANES, LANES)
            kern = conv_kernel[:, pl.ds(from_all, LANES)]
            total = jnp.zeros((LENGTH, LANES), jnp.float32)
            for tap in range(taps):
                begin = LEAD - (taps - 1) + tap
                total = total + kern[tap : tap + 1, :] * padded[begin : begin + LENGTH, cols]
            filtered[seq_rows(i), cols] = total
            return sums[0] + total, sums[1] + total * total

        zero = jnp.zeros((LENGTH, LANES), jnp.float32)
        one, two = lax.fori_loop(0, width // LANES, column, (zero, zero))
        lane = lax.broadcasted_iota(jnp.int32, (LENGTH, LANES), 1)
        both = jnp.where(
            lane == 0,
            jnp.sum(one, axis=-1, keepdims=True),
            jnp.where(lane == 1, jnp.sum(two, axis=-1, keepdims=True), 0.0),
        )
        own_stats[:, seq_rows(i)] = both.T[0:8, :]

    def stat_copies():
        copies = []
        for dr in range(reps):
            for dt in range(tps):
                if dr or dt:
                    copies.append(
                        pltpu.make_async_remote_copy(
                            src_ref=own_stats,
                            dst_ref=peer_stats.at[dr * tps + dt],
                            send_sem=stat_send.at[dr, dt],
                            recv_sem=stat_recv.at[dr, dt],
                            device_id={
                                "rep": lax.rem(rep + dr, reps),
                                "tp": lax.rem(tp + dt, tps),
                            },
                            device_id_type=MESH,
                        )
                    )
        return copies

    def activate_rows(i, carry):
        total = own_stats[:, seq_rows(i)]
        for k in range(1, reps * tps):
            total = total + peer_stats[k, :, seq_rows(i)]
        turned = jnp.concatenate([total] * (LANES // 8), axis=0).T
        mean = turned[:, 0:1] / channels
        variance = turned[:, 1:2] / channels - mean * mean
        gain_at = pl.multiple_of(tp * own_width + rep * width, LANES)
        gain = chan_gain[:, pl.ds(gain_at, width)]
        x = (filtered[seq_rows(i), :] - mean) * lax.rsqrt(variance + EPS) * gain
        activated[seq_rows(i), :] = (x / (1.0 + jnp.exp(-x))).astype(jnp.bfloat16)
        return carry

    def share(order, o, left, pieces_of, parts, peers, send, recv):
        span = pl.ds(pl.multiple_of(o * block, block), block)

        def one(i, carry):
            at = pl.ds(pl.multiple_of(i * rows, rows), rows)
            total = None
            for k, c in enumerate(pieces_of):
                term = times_transposed(
                    left[at, k * width : (k + 1) * width], weights[c, span, :]
                )
                total = term if total is None else total + term
            parts[o, at, :] = total.astype(jnp.bfloat16)
            return carry

        lax.fori_loop(0, reps, one, 0)
        keeper = o // per_tp
        dt = lax.rem(keeper + tps - tp, tps)
        waits = []
        for dr in [*range(1, reps), 0]:
            to = lax.rem(rep + dr, reps)
            copy = pltpu.make_async_remote_copy(
                src_ref=parts.at[o, pl.ds(pl.multiple_of(to * rows, rows), rows), :],
                dst_ref=peers.at[dr * tps + dt, lax.rem(o, per_tp)],
                send_sem=send.at[order, dr],
                recv_sem=recv.at[dr * tps + dt, lax.rem(o, per_tp)],
                device_id={"rep": to, "tp": keeper},
                device_id_type=MESH,
            )
            if dr:
                copy.start()
                waits.append(copy.wait_send)
            else:
                pl.when(keeper != tp)(copy.start)
                waits.append(lambda k=keeper, c=copy: pl.when(k != tp)(c.wait_send))
        return waits

    def wait_peers(j, parts, peers, send, recv):
        for k in range(1, reps * tps):
            dr, dt = k // tps, k % tps
            pltpu.make_async_remote_copy(
                src_ref=parts.at[0, own_rows, :],
                dst_ref=peers.at[k, j],
                send_sem=send.at[0, 0],
                recv_sem=recv.at[k, j],
                device_id={"rep": lax.rem(rep + dr, reps), "tp": lax.rem(tp + dt, tps)},
                device_id_type=MESH,
            ).wait_recv()

    def total_of(j, parts, peers):
        total = parts[tp * per_tp + j, own_rows, :].astype(jnp.float32)
        for k in range(1, reps * tps):
            total = total + peers[k, j].astype(jnp.float32)
        return total

    stepwise = blocks == n

    def owners(s):
        if s in (0, half_way):
            return [ring_index(place + s)]
        return [ring_index(place - s), ring_index(place + s)]

    def steps_of(c):
        return range(1, half_way + 1)

    first, second = (0, 1), (2, 3)
    third = tuple(range(4, 3 + ups))
    fourth = tuple(range(3 + ups, chunks))

    pump(0, 1)
    pump(1, 1)
    forward, finish = spread(states, rows_in, in_send, in_recv)
    padded[0:LEAD, :] = jnp.zeros((LEAD, width), jnp.float32)
    pump(0, 2)
    pump(1, 2)
    later = forward()
    for s in range(3, half_way + 1):
        pump(0, s)
        if s == 3:
            own_load.wait()
            finish(later)
        pump(1, s)
        if s == 3:
            norm_all(rows_in, mix_gain)
    pump(2, 1)
    pump(3, 1)
    arrived(0)
    arrived(1)

    todo = [(c, s) for s in range(2, half_way + 1) for c in second]

    def next_hop():
        if todo:
            pump(*todo.pop(0))

    for i in range(0, pieces, 2):
        lax.fori_loop(
            i, min(i + 2, pieces), lambda k, carry: (mixer_rows(k), carry)[1], 0
        )
        next_hop()
    stats = stat_copies()
    for one in stats:
        one.start()
    for one in stats:
        one.wait_recv()
    lax.fori_loop(0, pieces, activate_rows, 0)
    waits = []
    mix = (activated, (2,), mix_parts, mix_peers, mix_send, mix_recv)
    if stepwise:
        for s in range(half_way - 1):
            for o in owners(s):
                waits += share(len(waits) // reps, o, *mix)
    while todo:
        next_hop()
    if stepwise:
        for o in owners(half_way - 1):
            waits += share(len(waits) // reps, o, *mix)
    for c in third:
        pump(c, 1)
    arrived(2)
    if stepwise:
        waits += share(len(waits) // reps, owners(half_way)[0], *mix)
    else:
        for o in range(blocks):
            waits += share(o, o, *mix)

    todo = [(c, s) for s in range(2, half_way + 1) for c in third]
    for _ in range(len(todo) // 2):
        next_hop()
    for j in range(per_tp):
        wait_peers(j, mix_parts, mix_peers, mix_send, mix_recv)
        at = pl.ds(pl.multiple_of(tp * own_width + j * block, block), block)
        rows_mid[own_rows, at] = (
            rows_in[own_rows, at].astype(jnp.float32) + total_of(j, mix_parts, mix_peers)
        ).astype(jnp.bfloat16)
    forward, finish = spread(rows_mid.at[own_rows, own_cols], rows_mid, mid_send, mid_recv)
    while todo:
        next_hop()
    for c in fourth:
        pump(c, 1)
    arrived(3)
    for c in third:
        arrived(c)
    later = forward()
    finish(later)
    norm_all(rows_mid, mlp_gain)
    todo = [(c, s) for s in range(2, half_way + 1) for c in fourth]
    next_hop()
    for k in range(ups):

        def up_rows(i, carry):
            at = pl.ds(pl.multiple_of(i * rows, rows), rows)
            x = jnp.dot(normed[at, :], weights[3 + k], preferred_element_type=jnp.float32)
            x = jnp.maximum(x, 0.0)
            hidden[at, k * width : (k + 1) * width] = (x * x).astype(jnp.bfloat16)
            return carry

        lax.fori_loop(0, reps, up_rows, 0)
        next_hop()
    done = []
    fed = (hidden, fourth, fed_parts, fed_peers, fed_send, fed_recv)
    if stepwise:
        for o in owners(0):
            done += share(len(done) // reps, o, *fed)
    for s in range(2, half_way + 1):
        while todo and todo[0][1] <= s:
            next_hop()
        if stepwise:
            for o in owners(s - 1):
                done += share(len(done) // reps, o, *fed)
    for c in fourth:
        arrived(c)
    if stepwise:
        done += share(len(done) // reps, owners(half_way)[0], *fed)
    else:
        for o in range(blocks):
            done += share(o, o, *fed)
    for j in range(per_tp):
        wait_peers(j, fed_parts, fed_peers, fed_send, fed_recv)
        at = pl.ds(pl.multiple_of(tp * own_width + j * block, block), block)
        out[:, j * block : (j + 1) * block] = (
            rows_mid[own_rows, at].astype(jnp.float32) + total_of(j, fed_parts, fed_peers)
        ).astype(jnp.bfloat16)
    for one in stats:
        one.wait_send()
    for wait in waits + done:
        wait()


def body(mesh, states, mix_gain, w_value, w_gate, conv_kernel, chan_gain, w_mix, mlp_gain, w_up, w_down):
    reps, n, tps = mesh.shape["rep"], mesh.shape["fs"], mesh.shape["tp"]
    rows, own_width = states.shape
    width = own_width // reps
    channels = own_width * tps
    ups = w_up.shape[1] // own_width
    tokens = rows * reps
    group = reps * tps
    block = channels // n if channels // n >= LANES else own_width
    blocks, per_tp = channels // block, own_width // block
    chunks = 3 + 2 * ups
    bf16, f32 = jnp.bfloat16, jnp.float32
    vmem, hbm = pl.BlockSpec(memory_space=pltpu.VMEM), pl.BlockSpec(memory_space=pl.ANY)
    dma = pltpu.SemaphoreType.DMA
    return pl.pallas_call(
        functools.partial(kernel, (reps, n, tps, rows, channels, width, ups)),
        out_shape=jax.ShapeDtypeStruct((rows, own_width), bf16),
        in_specs=[hbm, vmem, hbm, hbm, vmem, vmem, hbm, vmem, hbm, hbm],
        out_specs=vmem,
        scratch_shapes=[
            pltpu.VMEM((chunks, channels, width), bf16),
            pltpu.VMEM((tokens, channels), bf16),
            pltpu.VMEM((tokens, channels), bf16),
            pltpu.VMEM((tokens, channels), bf16),
            pltpu.VMEM((LEAD + LENGTH, width), f32),
            pltpu.VMEM((tokens, width), f32),
            pltpu.VMEM((tokens, width), bf16),
            pltpu.VMEM((tokens, ups * width), bf16),
            pltpu.VMEM((8, tokens), f32),
            pltpu.VMEM((group, 8, tokens), f32),
            pltpu.VMEM((blocks, tokens, block), bf16),
            pltpu.VMEM((group, per_tp, rows, block), bf16),
            pltpu.VMEM((blocks, tokens, block), bf16),
            pltpu.VMEM((group, per_tp, rows, block), bf16),
            dma((chunks + 1,)),
            dma((2, chunks)),
            dma((2, chunks, n // 2)),
            dma((reps, tps)),
            dma((reps, tps)),
            dma((reps, tps)),
            dma((reps, tps)),
            dma((reps, tps)),
            dma((reps, tps)),
            dma((blocks, reps)),
            dma((group, per_tp)),
            dma((blocks, reps)),
            dma((group, per_tp)),
        ],
        compiler_params=pltpu.CompilerParams(
            collective_id=0, has_side_effects=True, vmem_limit_bytes=62 * 1024 * 1024
        ),
    )(
        states, mix_gain[None, :], w_value, w_gate, conv_kernel, chan_gain[None, :], w_mix,
        mlp_gain[None, :], w_up, w_down,
    )


def solution(mesh):
    in_specs = (
        P(("rep", "fs"), "tp"),
        P(),
        P("fs", "tp"),
        P("fs", "tp"),
        P(),
        P(),
        P("fs", "tp"),
        P(),
        P("fs", "tp"),
        P("fs", "tp"),
    )
    out_specs = P(("rep", "fs"), "tp")
    return jax.shard_map(
        functools.partial(body, mesh),
        mesh=mesh, in_specs=in_specs, out_specs=out_specs, check_vma=False,
    )
```

time: 619 us -> 196 us (0.32)
  waiting for transfers between devices: 540 us -> 0 us
  Pallas kernels: 0 us -> 193 us
  matrix products: 32.9 us -> 0 us
  other arithmetic: 17.6 us -> 0 us
  between operations: 13.4 us -> 0.01 us
    all_gather x9 -> x0, waiting for transfers between devices: 433 us -> none  [the longest x5 321 us: own_columns(): return lax.all_gather(piece, 'fs', axis=0, tiled=True)]
    pallas_call x0 -> x1, Pallas kernels: none -> 193 us  [body(): pl.pallas_call(functools.partial(kernel, (reps, n, tps, rows, channels, w...]
    reduce_scatter x4 -> x0, waiting for transfers between devices: 106 us -> none  [the longest x2 83.8 us: own_sums(): lax.psum_scatter(terms.astype(jnp.bfloat16), 'rep', scatter_dimension=0,...]
    dot_general x4 -> x0, matrix products: 32.9 us -> none  [the longest x2 22.4 us: times_transposed(): lax.dot_general(left, right, (((1,), (1,)), ((), ())), preferred_element_...]
    reduce_sum x3 -> x0, other arithmetic: 11.5 us -> none  [the longest x1 6.38 us: body(): jnp.sum(filtered, axis=-1)]
  transfers between devices with their start and end apart: 13 -> 0, of which waited for: 13 -> 0; matrix products, arithmetic and copies ran while one was open for 5% -> 0% of each run, Pallas kernels for 0% -> 0%
where the time goes in v2:
time: 196 us; the launch traced here: 195 us
  Pallas kernels  193 us (98%)
  local copies, waits for them, and re-layouts  2.06 us (1%)
    pallas_call x1, Pallas kernels, body(): pl.pallas_call(functools.partial(kernel, (reps, n, tps, rows, channels, w...  193 us

profile of v2, /device:TPU:0, one launch (start us, length us, event | category | flops | bytes accessed | tf_op | source)
XLA Modules:
  0.0 195.1 jit_solution(4096192617919736311)
XLA Ops:
  0.0 193.0 %shard_map.100 = bf16[384,1024]{1,0:T(8,128)(2,1)} custom-call(bf16[384,1024]{1,0:T(8,128)(2,1)} %states.1, f32[1,2048]{1,0:T(1,128)} %bitcast.3, bf16[256,1024]{1,0:T(8,128)(2,1)} %w_value.1, bf16[256,1024]{1,0:T(8,128)(2,1)} %w_gate.1, f32[31,2048]{1,0:T(8,128)} %conv_kernel.1, f32[1,2048]{1,0:T(1,128)} %bitcast.4, bf16[256,1024]{1,0:T(8,128)(2,1)} %w_mix.1, ...), custom_call_target="tpu_custom_call" | custom-call | tf_op jit(solution)/shard_map/pallas_call | solution.py:437
  193.0 2.1 %copy.12 = bf16[384,1024]{1,0:T(8,128)(2,1)} copy(bf16[384,1024]{1,0:T(8,128)(2,1)} %shard_map.100) | data formatting | bytes 1572864

commit v3 on v2

--- a/solution.py
+++ b/solution.py
@@ -59,7 +59,6 @@
                     device_id={"rep": lax.rem(rep + dr, reps), "tp": lax.rem(tp + dt, tps)},
                     device_id_type=MESH,
                 )
-    pl.semaphore_wait(barrier, 1 + reps * tps)
 
     own_rows = pl.ds(pl.multiple_of(rep * rows, rows), rows)
     own_cols = pl.ds(pl.multiple_of(tp * own_width, own_width), own_width)
@@ -101,6 +100,7 @@
         loads[-1].start()
     own_load = pltpu.make_async_copy(states, rows_in.at[own_rows, own_cols], load_sems.at[chunks])
     own_load.start()
+    pl.semaphore_wait(barrier, 1 + reps * tps)
 
     def pump(c, s):
         for way in range(2):
@@ -235,7 +235,7 @@
     def share(order, o, left, pieces_of, parts, peers, send, recv):
         span = pl.ds(pl.multiple_of(o * block, block), block)
 
-        def one(i, carry):
+        def one(i):
             at = pl.ds(pl.multiple_of(i * rows, rows), rows)
             total = None
             for k, c in enumerate(pieces_of):
@@ -244,14 +244,13 @@
                 )
                 total = term if total is None else total + term
             parts[o, at, :] = total.astype(jnp.bfloat16)
-            return carry
-
-        lax.fori_loop(0, reps, one, 0)
+
         keeper = o // per_tp
         dt = lax.rem(keeper + tps - tp, tps)
         waits = []
         for dr in [*range(1, reps), 0]:
             to = lax.rem(rep + dr, reps)
+            one(to)
             copy = pltpu.make_async_remote_copy(
                 src_ref=parts.at[o, pl.ds(pl.multiple_of(to * rows, rows), rows), :],
                 dst_ref=peers.at[dr * tps + dt, lax.rem(o, per_tp)],

time: 196 us -> 195 us (level)
  no operation moved by 1% of the time
where the time goes in v3:
time: 195 us
  Pallas kernels  193 us (99%)
  local copies, waits for them, and re-layouts  2.06 us (1%)
    pallas_call x1, Pallas kernels, body(): pl.pallas_call(functools.partial(kernel, (reps, n, tps, rows, channels, w...  193 us

profile of v3, /device:TPU:0, one launch (start us, length us, event | category | flops | bytes accessed | tf_op | source)
XLA Modules:
  0.0 194.7 jit_solution(10029835219497245322)
XLA Ops:
  0.0 192.6 %shard_map.100 = bf16[384,1024]{1,0:T(8,128)(2,1)} custom-call(bf16[384,1024]{1,0:T(8,128)(2,1)} %states.1, f32[1,2048]{1,0:T(1,128)} %bitcast.3, bf16[256,1024]{1,0:T(8,128)(2,1)} %w_value.1, bf16[256,1024]{1,0:T(8,128)(2,1)} %w_gate.1, f32[31,2048]{1,0:T(8,128)} %conv_kernel.1, f32[1,2048]{1,0:T(1,128)} %bitcast.4, bf16[256,1024]{1,0:T(8,128)(2,1)} %w_mix.1, ...), custom_call_target="tpu_custom_call" | custom-call | tf_op jit(solution)/shard_map/pallas_call | solution.py:436
  192.6 2.1 %copy.12 = bf16[384,1024]{1,0:T(8,128)(2,1)} copy(bf16[384,1024]{1,0:T(8,128)(2,1)} %shard_map.100) | data formatting | bytes 1572864
